TPU v7x, 32 devices: a whole 2x2x4 slice. The times are simulated.
32 devices in a mesh: ep: 8 (over z, x), tp: 4 (over y, core).
Axes of the slice: x: 2, y: 2, z: 4, core: 2. Of those that a mesh axis runs over, the one named last changes fastest.
Arguments:
- tokens: bfloat16 [128, 2048], P('ep'), may hold values from -6 to 6
- norm1_gain: float32 [2048], replicated, may hold values from 0.1 to 1.9
- query_weight: bfloat16 [2048, 512], P(None, 'tp'), may hold values from -0.125 to 0.125
- key_weight: bfloat16 [2048, 256], P(None, 'tp'), may hold values from -0.125 to 0.125
- value_weight: bfloat16 [2048, 256], P(None, 'tp'), may hold values from -0.125 to 0.125
- forget_weight: bfloat16 [2048, 8], P(None, 'tp'), may hold values from -0.125 to 0.125
- forget_bias: float32 [8], P('tp'), may hold values from 0.5 to 4
- out_weight: bfloat16 [512, 2048], P('tp'), may hold values from -0.25 to 0.25
- kv_cache: bfloat16 [128, 1024, 4, 128], P('ep', None, 'tp'), may hold values from -6 to 6
- log_gates: float32 [128, 8, 1024], P('ep', 'tp'), may hold values from -1024 to 0, as said below
- lengths: int32 [128], P('ep'), may hold values from 64 to 1024
- norm2_gain: float32 [2048], replicated, may hold values from 0.1 to 1.9
- routing: int32 [128, 4], P('ep'), may hold values from 0 to 7, all different within a row; in each aligned block of 16 rows (0 to 15, 16 to 31, ...) at most 16 rows name the same one
- route_weight: float32 [128, 4], P('ep'), may hold values from 0.1 to 0.6
- expert_gate: bfloat16 [8, 2048, 2048], P('ep', None, 'tp'), may hold values from -0.25 to 0.25
- expert_up: bfloat16 [8, 2048, 2048], P('ep', None, 'tp'), may hold values from -0.25 to 0.25
- expert_down: bfloat16 [8, 2048, 2048], P('ep', 'tp'), may hold values from -0.0625 to 0.0625
- dense_gate: bfloat16 [2048, 4096], P(None, 'ep'), may hold values from -0.25 to 0.25
- dense_up: bfloat16 [2048, 4096], P(None, 'ep'), may hold values from -0.25 to 0.25
- dense_down: bfloat16 [4096, 2048], P('ep'), may hold values from -0.09375 to 0.09375
- dense_mix: float32 [2048], replicated, may hold values from -0.125 to 0.125
Outputs:
- layer_out: bfloat16 [128, 2048], P(('ep', 'tp'))
Inputs may be any that keep to these rules, and one draw needn't show every extreme that they name: `log_gates`: Non-increasing along the positions. `routing`: each row names 4 different experts. Among the rows of one index of ep (aligned blocks of 16 rows) no expert is named by more than 16 rows, and in every draw some expert is named by exactly 16 rows of some block.
All inputs are finite; a program needn't handle non-finite values.
Results may differ from a plain program's by a relative error of at most 0.011.
Values may be sent and summed in bfloat16 or wider, within the bound.
No kernel may reach another device: no remote copies, remote signals or barrier semaphores. Data moves between devices by JAX's collectives and lax.ppermute only.
A program may use at most 128 MiB of HBM per device.

v0:
```python
import jax
import jax.numpy as jnp
from jax import lax
from jax.sharding import PartitionSpec as P

EPS = 1e-05
LIMIT = 7.0
ALPHA = 1.702


def clamped_unit(gate_pre, up_pre):
    capped = jnp.minimum(gate_pre, LIMIT)
    return capped * jax.nn.sigmoid(ALPHA * capped) * (jnp.clip(up_pre, -LIMIT, LIMIT) + 1.0)


def rms_scaled(values, gain_vec):
    return values * lax.rsqrt(jnp.mean(values * values, axis=-1, keepdims=True) + EPS) * gain_vec


def slot_tables(routes, experts, capacity):
    flat_ids = routes.reshape(-1)
    onehot = (flat_ids[:, None] == jnp.arange(experts, dtype=jnp.int32)[None, :]).astype(jnp.int32)
    earlier = jnp.cumsum(onehot, axis=0, dtype=jnp.int32) - onehot
    slot_ids = jnp.sum(earlier * onehot, axis=1, dtype=jnp.int32)
    matches = onehot[:, :, None] * (
        slot_ids[:, None, None] == jnp.arange(capacity, dtype=jnp.int32)[None, None, :]
    ).astype(jnp.int32)
    owners = jnp.arange(flat_ids.shape[0], dtype=jnp.int32) // routes.shape[1]
    source = jnp.sum(matches * owners[:, None, None], axis=0, dtype=jnp.int32)
    return (slot_ids, source)


def on_device(
    tokens,
    norm1_gain,
    query_weight,
    key_weight,
    value_weight,
    forget_weight,
    forget_bias,
    out_weight,
    kv_cache,
    log_gates,
    lengths,
    norm2_gain,
    routing,
    route_weight,
    expert_gate,
    expert_up,
    expert_down,
    dense_gate,
    dense_up,
    dense_down,
    dense_mix,
):
    seq_count, model_width = tokens.shape
    tp_count = lax.axis_size("tp")
    ep_count = lax.axis_size("ep")
    own_rows = seq_count // tp_count
    row_start = lax.axis_index("tp") * own_rows
    local_heads = forget_bias.shape[0]
    kv_local = kv_cache.shape[2]
    head_dim = kv_cache.shape[3] // 2
    per_kv = local_heads // kv_local
    cache_len = kv_cache.shape[1]
    score_scale = head_dim ** (-0.5)
    normed = rms_scaled(tokens.astype(jnp.float32), norm1_gain).astype(jnp.bfloat16)
    queries = jnp.dot(normed, query_weight, preferred_element_type=jnp.float32).astype(jnp.bfloat16)
    queries = queries.reshape(seq_count, kv_local, per_kv, head_dim)
    key_new = jnp.dot(normed, key_weight, preferred_element_type=jnp.float32).astype(jnp.bfloat16)
    key_new = key_new.reshape(seq_count, kv_local, head_dim)
    value_new = jnp.dot(normed, value_weight, preferred_element_type=jnp.float32).astype(
        jnp.bfloat16
    )
    value_new = value_new.reshape(seq_count, kv_local, head_dim)
    gate_new = jax.nn.log_sigmoid(
        jnp.dot(normed, forget_weight, preferred_element_type=jnp.float32) + forget_bias
    )
    scores = (
        jnp.einsum(
            "skgd,slkd->skgl", queries, kv_cache[..., :head_dim], preferred_element_type=jnp.float32
        )
        * score_scale
    )
    last_index = jnp.broadcast_to((lengths - 1)[:, None, None], (seq_count, local_heads, 1))
    last_gate = jnp.take_along_axis(log_gates, last_index, axis=2)
    gate_bias = (last_gate - log_gates + gate_new[:, :, None]).reshape(
        seq_count, kv_local, per_kv, cache_len
    )
    live_mask = (jnp.arange(cache_len, dtype=jnp.int32)[None, :] < lengths[:, None])[
        :, None, None, :
    ]
    cached = jnp.where(live_mask, jnp.exp(scores + gate_bias), 0.0)
    own_exp = jnp.exp(
        jnp.einsum("skgd,skd->skg", queries, key_new, preferred_element_type=jnp.float32)
        * score_scale
    )
    denominator = jnp.sum(cached, axis=-1) + own_exp
    weight_cache = (cached / denominator[..., None]).astype(jnp.bfloat16)
    weight_own = (own_exp / denominator).astype(jnp.bfloat16)
    attended = jnp.einsum(
        "skgl,slkd->skgd",
        weight_cache,
        kv_cache[..., head_dim:],
        preferred_element_type=jnp.float32,
    )
    attended = (
        attended
        + weight_own.astype(jnp.float32)[..., None] * value_new.astype(jnp.float32)[:, :, None, :]
    )
    attended = attended.astype(jnp.bfloat16).reshape(seq_count, local_heads * head_dim)
    partial_out = jnp.dot(attended, out_weight, preferred_element_type=jnp.float32)
    attn_out = lax.psum(partial_out, "tp").astype(jnp.bfloat16)
    residual = tokens.astype(jnp.float32) + attn_out.astype(jnp.float32)
    hidden_in = rms_scaled(residual, norm2_gain).astype(jnp.bfloat16)
    own_hidden = lax.dynamic_slice_in_dim(hidden_in, row_start, own_rows, 0)
    own_residual = lax.dynamic_slice_in_dim(residual, row_start, own_rows, 0)
    row_piece = lax.all_gather(own_hidden, "ep", axis=0, tiled=True)
    gate_pre = jnp.dot(row_piece, dense_gate, preferred_element_type=jnp.float32)
    up_pre = jnp.dot(row_piece, dense_up, preferred_element_type=jnp.float32)
    dense_act = clamped_unit(gate_pre, up_pre).astype(jnp.bfloat16)
    dense_val = lax.psum_scatter(
        jnp.dot(dense_act, dense_down, preferred_element_type=jnp.float32),
        "ep",
        scatter_dimension=0,
        tiled=True,
    )
    local_experts = expert_gate.shape[0]
    experts = local_experts * ep_count
    top_count = routing.shape[1]
    capacity = min(seq_count, seq_count * top_count * 3 // experts)
    slot_ids, source = slot_tables(routing, experts, capacity)
    dispatch = hidden_in[source.reshape(-1)].reshape(experts, capacity, model_width)
    received = lax.all_to_all(dispatch, "ep", split_axis=0, concat_axis=0, tiled=True)
    item_count = received.shape[1]
    grouped = received.reshape(ep_count, local_experts, item_count, model_width)
    gate_pre = jnp.einsum(
        "sjnd,jdf->sjnf", grouped, expert_gate, preferred_element_type=jnp.float32
    )
    up_pre = jnp.einsum("sjnd,jdf->sjnf", grouped, expert_up, preferred_element_type=jnp.float32)
    activation = clamped_unit(gate_pre, up_pre).astype(jnp.bfloat16)
    partial_units = jnp.einsum(
        "sjnf,jfd->sjnd", activation, expert_down, preferred_element_type=jnp.float32
    )
    partial_units = partial_units.reshape(ep_count * local_experts, item_count, model_width)
    slot_index = routing * capacity + slot_ids.reshape(seq_count, top_count)
    shares = lax.psum_scatter(
        partial_units.astype(jnp.bfloat16), "tp", scatter_dimension=2, tiled=True
    )
    returned = lax.all_to_all(shares, "ep", split_axis=0, concat_axis=0, tiled=True)
    share_width = returned.shape[2]
    picked = returned.reshape(experts * capacity, share_width)[slot_index.reshape(-1)]
    picked = picked.reshape(seq_count, top_count, share_width)
    moe_cols = jnp.sum(route_weight[..., None] * picked.astype(jnp.float32), axis=1)
    moe_val = lax.all_to_all(
        moe_cols.astype(jnp.bfloat16), "tp", split_axis=0, concat_axis=1, tiled=True
    ).astype(moe_cols.dtype)
    mix_gate = jax.nn.sigmoid(
        jnp.dot(own_hidden.astype(jnp.float32), dense_mix, precision=lax.Precision.HIGHEST)
    )
    return (own_residual + moe_val + mix_gate[:, None] * dense_val).astype(jnp.bfloat16)


def solution(mesh):
    return jax.shard_map(
        on_device,
        mesh=mesh,
        in_specs=(
            P("ep", None),
            P(),
            P(None, "tp"),
            P(None, "tp"),
            P(None, "tp"),
            P(None, "tp"),
            P("tp"),
            P("tp", None),
            P("ep", None, "tp", None),
            P("ep", "tp", None),
            P("ep"),
            P(),
            P("ep", None),
            P("ep", None),
            P("ep", None, "tp"),
            P("ep", None, "tp"),
            P("ep", "tp", None),
            P(None, "ep"),
            P(None, "ep"),
            P("ep", None),
            P(),
        ),
        out_specs=P(("ep", "tp"), None),
        check_vma=False,
    )
```

profile of v0, /device:TPU:0, one launch (start us, length us, event | category | flops | bytes accessed | tf_op | source)
XLA Modules:
  0.0 175.3 jit_solution(10059559181539150195)
XLA Ops:
  7.4 0.8 broadcast_add_fusion
  8.2 0.7 broadcast_compare_fusion
  8.8 0.7 iota_compare_fusion
  9.6 0.1 copy.44
  9.7 0.1 reshape.457
  9.8 0.0 copy-start.4
  9.8 0.0 copy-start.5
  9.9 0.0 copy-start.10
  9.9 0.0 copy-start.11
  9.9 1.8 %gather_fusion.2 = f32[32]{0:T(128)S(1)} fusion(f32[16,2,1024]{2,1,0:T(2,128)} %param.30, s32[32]{0:T(128)S(1)} %reshape.457), kind=kCustom, calls=%fused_computation.2 | custom fusion | bytes 640 | tf_op jit(solution)/shard_map/jit(take_along_axis)/gather | solution.py:86
  11.7 0.1 gather.13
  11.8 0.1 fusion.97
  11.9 0.0 copy-done.2
  11.9 0.1 fusion.72
  12.1 0.2 convolution_convert_fusion.3
  12.3 0.1 reshape.424
  12.4 0.2 fusion.102
  12.6 0.1 copy.45
  12.7 0.2 fusion.55
  12.9 0.2 fusion.54
  13.2 0.1 fusion.98
  13.3 3.6 %fusion.123 = (f32[16,2]{1,0:T(8,128)S(1)}, f32[16,2,1024]{2,1,0:T(2,128)S(1)}) fusion(f32[16,2]{1,0:T(8,128)S(1)} %copy.45, f32[16,2,1024]{2,1,0:T(2,128)S(1)} %copy-done.1, f32[16,2]{1,0:T(8,128)S(1)} %fusion.97, bf16[16,2,64]{2,1,0:T(2,128)(2,1)S(1)} %reshape.424, bf16[16,1024,1,128]{3,1,2,0:T(8,128)(2,1)} %param.29, ...), kind=kOutput, calls=%fused_computation.138 | convolution fusion | flops 4390880 | bytes 4477312 | tf_op jit(solution)/shard_map/skgd,slkd->skgl/dot_general | solution.py:80
  17.0 0.0 copy-start.7
  17.0 1.4 fusion.51
  18.4 0.1 reshape.427
  18.5 0.2 fusion.124
  18.7 14.5 %all-reduce.5 = bf16[16,2048]{1,0:T(8,128)(2,1)S(1)} all-reduce(f32[16,2048]{1,0:T(8,128)S(1)} %fusion.124), channel_id=1, replica_groups=mesh['ep'=8,'tp'=4] {'tp'}, use_global_device_ids=true, to_apply=%region_2.3 | all-reduce | flops 32768 | bytes 196608 | tf_op jit(solution)/shard_map/psum | solution.py:113
  33.2 0.1 multiply_reduce_fusion.1
  33.3 0.1 copy.48
  33.4 0.1 eq.37
  33.5 0.1 fusion.93
  33.6 0.1 copy.49
  33.7 0.1 reduce_window_sum.11
  33.8 0.2 select_reduce_fusion
  34.0 0.2 multiply_reduce_fusion.2
  34.2 0.1 reshape.428
  34.3 0.1 multiply_convert_fusion
  34.4 0.9 gather_fusion
  35.3 19.1 %all_to_all.20 = bf16[8,16,2048]{2,1,0:T(8,128)(2,1)S(1)} all-to-all(bf16[8,16,2048]{2,1,0:T(8,128)(2,1)S(1)} %bitcast.124), channel_id=1, replica_groups=mesh['ep'=8,'tp'=4] {'ep'}, dimensions={0} | all-to-all | bytes 1048576 | tf_op jit(solution)/shard_map/all_to_all | solution.py:134
  54.4 2.0 %fusion.14 = f32[8,1,16,512]{3,2,0,1:T(8,128)S(1)} fusion(bf16[8,16,2048]{2,1,0:T(8,128)(2,1)S(1)} %all_to_all.20, bf16[1,2048,512]{2,1,0:T(8,128)(2,1)} %param.35), kind=kOutput, calls=%fused_computation.16 | convolution fusion | flops 268500992 | bytes 2883584 | tf_op jit(solution)/shard_map/sjnd,jdf->sjnf/dot_general | solution.py:137
  56.4 3.2 %convolution_convert_fusion = bf16[8,16,2048]{2,1,0:T(8,128)(2,1)} fusion(bf16[1,512,2048]{2,1,0:T(8,128)(2,1)S(1)} %copy-done, bf16[8,16,2048]{2,1,0:T(8,128)(2,1)S(1)} %all_to_all.20, bf16[1,2048,512]{2,1,0:T(8,128)(2,1)} %param.36, f32[8,1,16,512]{3,2,0,1:T(8,128)S(1)} %fusion.14), kind=kOutput, calls=%fused_computation.9 | convolution fusion | flops 537722880 | bytes 5505024 | tf_op jit(solution)/shard_map/sjnf,jfd->sjnd/dot_general | solution.py:142
  59.6 0.0 reduce-scatter.2.cloned.1.call-update
  59.7 0.0 all-reduce.4.cloned.1.call-start
  59.8 30.5 %all-gather = bf16[8,4,2048]{2,1,0:T(4,128)(2,1)S(1)} all-gather(bf16[1,4,2048]{2,1,0:T(4,128)(2,1)S(1)} %dynamic-slice_bitcast_fusion), channel_id=1, replica_groups=mesh['ep'=8,'tp'=4] {'ep'}, dimensions={0}, use_global_device_ids=true | all-gather | bytes 147456 | tf_op jit(solution)/shard_map/all_gather | solution.py:118
  90.3 2.0 %convolution_minimum_fusion = f32[32,512]{1,0:T(8,128)S(1)} fusion(bf16[32,2048]{1,0:T(8,128)(2,1)S(1)} %reshape.466, bf16[2048,512]{1,0:T(8,128)(2,1)} %param.38), kind=kOutput, calls=%fused_computation.29 | convolution fusion | flops 67125248 | bytes 2293760 | tf_op jit(solution)/shard_map/dot_general | solution.py:119
  92.4 0.0 copy-start.8
  92.4 0.0 copy-start.15
  92.4 3.9 %fusion.47 = f32[32,2048]{1,0:T(8,128)} fusion(bf16[512,2048]{1,0:T(8,128)(2,1)} %param.40, bf16[32,2048]{1,0:T(8,128)(2,1)S(1)} %reshape.466, bf16[2048,512]{1,0:T(8,128)(2,1)} %param.39, f32[32,512]{1,0:T(8,128)S(1)} %convolution_minimum_fusion), kind=kOutput, calls=%fused_computation.31 | convolution fusion | flops 134365184 | bytes 4653056 | tf_op jit(solution)/shard_map/dot_general | solution.py:123
  96.3 0.0 all-reduce.4.cloned.1.call-update
  96.3 0.1 reshape.435
  96.4 0.1 reshape.436
  96.5 0.1 copy.47
  96.6 3.6 %all-to-all-start.1 = ((bf16[8,16,512]{2,1,0:T(8,128)(2,1)}), bf16[8,16,512]{2,1,0:T(8,128)(2,1)S(1)}, u32[]{:S(2)}, u32[]{:S(2)}) async-start(bf16[8,16,512]{2,1,0:T(8,128)(2,1)} %reduce-scatter.2.cloned.1.call-done), calls=%async_computation.2 | async-start | bytes 262144 | tf_op jit(solution)/shard_map/all_to_all | solution.py:150
  100.2 7.5 %all-to-all-done.1 = bf16[8,16,512]{2,1,0:T(8,128)(2,1)S(1)} async-done(((bf16[8,16,512]{2,1,0:T(8,128)(2,1)}), bf16[8,16,512]{2,1,0:T(8,128)(2,1)S(1)}, u32[]{:S(2)}, u32[]{:S(2)}) %all-to-all-start.1) | async-done | bytes 131104 | tf_op jit(solution)/shard_map/all_to_all | solution.py:150
  107.7 0.7 gather_fusion.1
  108.5 0.2 multiply_reduce_fusion
  108.6 0.6 convert_element_type.115
  109.2 3.3 %all-to-all-start.2 = ((bf16[4,4,512]{2,1,0:T(4,128)(2,1)}), bf16[4,4,512]{2,1,0:T(4,128)(2,1)S(1)}, u32[]{:S(2)}, u32[]{:S(2)}) async-start(bf16[4,4,512]{2,1,0:T(4,128)(2,1)} %convert_element_type.115), calls=%async_computation.3 | async-start | bytes 32768 | tf_op jit(solution)/shard_map/all_to_all | solution.py:155
  112.5 0.1 fusion.60
  112.6 0.1 copy-done.15
  112.7 0.6 dynamic-slice
  113.9 2.5 %all-to-all-done.2 = bf16[4,4,512]{2,1,0:T(4,128)(2,1)S(1)} async-done(((bf16[4,4,512]{2,1,0:T(4,128)(2,1)}), bf16[4,4,512]{2,1,0:T(4,128)(2,1)S(1)}, u32[]{:S(2)}, u32[]{:S(2)}) %all-to-all-start.2) | async-done | bytes 16416 | tf_op jit(solution)/shard_map/all_to_all | solution.py:155
  116.3 50.0 %all-reduce.4.cloned.1.call-done = f32[32,2048]{1,0:T(8,128)} async-done(((f32[32,2048]{1,0:T(8,128)}), f32[32,2048]{1,0:T(8,128)}) %all-reduce.4.cloned.1.call-update) | async-done | bytes 262160
  166.4 1.5 fusion.88
  (44 shorter events, 0.3 us)
Async XLA Ops:
  7.4 49.1 %copy-start = (bf16[1,512,2048]{2,1,0:T(8,128)(2,1)S(1)}, bf16[1,512,2048]{2,1,0:T(8,128)(2,1)}, u32[]{:S(2)}) copy-start(bf16[1,512,2048]{2,1,0:T(8,128)(2,1)} %param.37) | copy-start | bytes 6291460
  7.4 89.2 %reduce-scatter.2.cloned.1.call-start = ((), (), s32[]{:S(2)}) async-start(), calls=%async_computation.4 | async-start | bytes 655360 | tf_op jit(solution)/shard_map/reduce_scatter | solution.py:147
  9.8 2.1 %copy-start.2 = (bf16[16,2048]{1,0:T(8,128)(2,1)S(1)}, bf16[16,2048]{1,0:T(8,128)(2,1)}, u32[]{:S(2)}) copy-start(bf16[16,2048]{1,0:T(8,128)(2,1)} %param.21) | copy-start | bytes 196612
  9.8 2.2 %copy-start.4 = (bf16[2048,128]{1,0:T(8,128)(2,1)S(1)}, bf16[2048,128]{1,0:T(8,128)(2,1)}, u32[]{:S(2)}) copy-start(bf16[2048,128]{1,0:T(8,128)(2,1)} %param.23) | copy-start | bytes 1572868
  9.8 2.2 %copy-start.5 = (f32[2048]{0:T(1024)S(1)}, f32[2048]{0:T(1024)}, u32[]{:S(2)}) copy-start(f32[2048]{0:T(1024)} %param.22) | copy-start | bytes 24580
  9.9 2.5 %copy-start.12 = (bf16[2048,2]{0,1:T(2,128)(2,1)S(1)}, bf16[2048,2]{0,1:T(2,128)(2,1)}, u32[]{:S(2)}) copy-start(bf16[2048,2]{0,1:T(2,128)(2,1)} %param.26) | copy-start | bytes 24580
  9.9 2.5 %copy-start.14 = (f32[2]{0:T(128)S(1)}, f32[2]{0:T(128)}, u32[]{:S(2)}) copy-start(f32[2]{0:T(128)} %param.27) | copy-start | bytes 28
  9.9 2.8 %copy-start.10 = (bf16[2048,64]{0,1:T(8,128)(2,1)S(1)}, bf16[2048,64]{0,1:T(8,128)(2,1)}, u32[]{:S(2)}) copy-start(bf16[2048,64]{0,1:T(8,128)(2,1)} %param.24) | copy-start | bytes 786436
  9.9 3.0 %copy-start.11 = (bf16[2048,64]{0,1:T(8,128)(2,1)S(1)}, bf16[2048,64]{0,1:T(8,128)(2,1)}, u32[]{:S(2)}) copy-start(bf16[2048,64]{0,1:T(8,128)(2,1)} %param.25) | copy-start | bytes 786436
  9.9 3.4 %copy-start.1 = (f32[16,2,1024]{2,1,0:T(2,128)S(1)}, f32[16,2,1024]{2,1,0:T(2,128)}, u32[]{:S(2)}) copy-start(f32[16,2,1024]{2,1,0:T(2,128)} %param.30) | copy-start | bytes 393220
  13.3 3.7 %copy-start.9 = (bf16[16,1024,1,128]{3,1,2,0:T(8,128)(2,1)S(1)}, bf16[16,1024,1,128]{3,1,2,0:T(8,128)(2,1)}, u32[]{:S(2)}) copy-start(bf16[16,1024,1,128]{3,1,2,0:T(8,128)(2,1)} %param.29) | copy-start | bytes 12582916
  17.0 1.5 copy-start.3
  17.0 16.3 %copy-start.7 = (s32[16,4]{0,1:T(4,128)S(1)}, s32[16,4]{0,1:T(4,128)}, u32[]{:S(2)}) copy-start(s32[16,4]{0,1:T(4,128)} %param.33) | copy-start | bytes 772
  17.0 17.3 %copy-start.6 = (f32[2048]{0:T(1024)S(1)}, f32[2048]{0:T(1024)}, u32[]{:S(2)}) copy-start(f32[2048]{0:T(1024)} %param.32) | copy-start | bytes 24580
  59.7 106.7 %all-reduce.4.cloned.1.call-start = ((), (), s32[]{:S(2)}) async-start(), calls=%async_computation.5 | async-start | bytes 524288
  92.4 4.1 %copy-start.8 = (f32[16,4]{0,1:T(4,128)S(1)}, f32[16,4]{0,1:T(4,128)}, u32[]{:S(2)}) copy-start(f32[16,4]{0,1:T(4,128)} %param.34) | copy-start | bytes 772
  92.4 20.1 %copy-start.13 = (f32[2048]{0:T(1024)S(1)}, f32[2048]{0:T(1024)}, u32[]{:S(2)}) copy-start(f32[2048]{0:T(1024)} %param.41) | copy-start | bytes 24580
  92.4 20.3 %copy-start.15 = (u32[32]{0:T(128)S(1)}, u32[32]{0:T(128)}, u32[]{:S(2)}) copy-start(u32[32]{0:T(128)} %constant.108) | copy-start | bytes 388
  96.6 11.1 %all-to-all-start.1 = ((bf16[8,16,512]{2,1,0:T(8,128)(2,1)}), bf16[8,16,512]{2,1,0:T(8,128)(2,1)S(1)}, u32[]{:S(2)}, u32[]{:S(2)}) async-start(bf16[8,16,512]{2,1,0:T(8,128)(2,1)} %reduce-scatter.2.cloned.1.call-done), calls=%async_computation.2 | async-start | bytes 262144 | tf_op jit(solution)/shard_map/all_to_all | solution.py:150
  109.2 7.1 %all-to-all-start.2 = ((bf16[4,4,512]{2,1,0:T(4,128)(2,1)}), bf16[4,4,512]{2,1,0:T(4,128)(2,1)S(1)}, u32[]{:S(2)}, u32[]{:S(2)}) async-start(bf16[4,4,512]{2,1,0:T(4,128)(2,1)} %convert_element_type.115), calls=%async_computation.3 | async-start | bytes 32768 | tf_op jit(solution)/shard_map/all_to_all | solution.py:155
Sparse Core Ops, SparseCore 0:
  59.8 20.9 reduce-scatter.1
Sparse Core Ops, SparseCore 1:
  96.4 69.9 all-reduce.3
where the time goes:
time: 176 us; the launch traced here: 175 us
  blocking collectives  64.1 us (36%)
  waiting for transfers between devices  60 us (34%)
  matrix products  17.5 us (10%)
  between operations  15.8 us (9%)
  starting transfers between devices  6.94 us (4%)
  local copies, waits for them, and re-layouts  6 us (3%)
  other arithmetic  4.98 us (3%)
    unnamed x3, waiting for transfers between devices  50.1 us
    all_gather x1, blocking collectives, on_device(): row_piece = lax.all_gather(own_hidden, 'ep', axis=0, tiled=True)  30.5 us
    all_to_all x1, blocking collectives, on_device(): lax.all_to_all(dispatch, 'ep', split_axis=0, concat_axis=0, tiled=True)  19.1 us
    psum x1, blocking collectives, on_device(): attn_out = lax.psum(partial_out, 'tp').astype(jnp.bfloat16)  14.5 us
    all_to_all x1, waiting for transfers between devices, on_device(): lax.all_to_all(shares, 'ep', split_axis=0, concat_axis=0, tiled=True)  7.48 us
    dot_general x1, matrix products, on_device(): jnp.dot(dense_act, dense_down, preferred_element_type=jnp.float32)  3.85 us
    all_to_all x1, starting transfers between devices, on_device(): lax.all_to_all(shares, 'ep', split_axis=0, concat_axis=0, tiled=True)  3.64 us
    dot_general x1, matrix products, on_device(): jnp.einsum('skgd,slkd->skgl', queries, kv_cache[..., :head_dim], preferre...  3.63 us
  transfers between devices with their start and end apart: 4, of which 3 were waited for; matrix products, arithmetic and copies ran while one was open for 5% of the time, Pallas kernels for 0%

commit v1 on v0

--- a/solution.py
+++ b/solution.py
@@ -115,7 +115,9 @@
     hidden_in = rms_scaled(residual, norm2_gain).astype(jnp.bfloat16)
     own_hidden = lax.dynamic_slice_in_dim(hidden_in, row_start, own_rows, 0)
     own_residual = lax.dynamic_slice_in_dim(residual, row_start, own_rows, 0)
-    row_piece = lax.all_gather(own_hidden, "ep", axis=0, tiled=True)
+    row_piece = jnp.concatenate(
+        lax.all_to_all(jnp.stack([own_hidden] * lax.axis_size("ep")), "ep", 0, 0), axis=0
+    )
     gate_pre = jnp.dot(row_piece, dense_gate, preferred_element_type=jnp.float32)
     up_pre = jnp.dot(row_piece, dense_up, preferred_element_type=jnp.float32)
     dense_act = clamped_unit(gate_pre, up_pre).astype(jnp.bfloat16)

time: 176 us -> 172 us (0.977)
  blocking collectives: 64.1 us -> 14.5 us
  waiting for transfers between devices: 60 us -> 92.7 us
  starting transfers between devices: 6.94 us -> 18.3 us
    all_gather x1 -> x0, blocking collectives: 30.5 us -> none  [on_device(): row_piece = lax.all_gather(own_hidden, 'ep', axis=0, tiled=True)]
    all_to_all x0 -> x2, waiting for transfers between devices: none -> 20.4 us  [the longest x1 13.4 us: on_device(): lax.all_to_all(dispatch, 'ep', split_axis=0, concat_axis=0, tiled=True)]
    all_to_all x1 -> x0, blocking collectives: 19.1 us -> none  [on_device(): lax.all_to_all(dispatch, 'ep', split_axis=0, concat_axis=0, tiled=True)]
    all_to_all x0 -> x2, starting transfers between devices: none -> 9.49 us  [the longest x1 5.81 us: on_device(): lax.all_to_all(dispatch, 'ep', split_axis=0, concat_axis=0, tiled=True)]
    unnamed x3, waiting for transfers between devices: 50.1 us -> 59.2 us
    reduce_scatter x1, waiting for transfers between devices: 0.01 us -> 7.28 us  [on_device(): lax.psum_scatter(partial_units.astype(jnp.bfloat16), 'tp', scatter_dimens...]
    all_to_all x1, waiting for transfers between devices: 7.48 us -> 3.42 us  [on_device(): lax.all_to_all(shares, 'ep', split_axis=0, concat_axis=0, tiled=True)]
    all_to_all x1, starting transfers between devices: 3.64 us -> 5.51 us  [on_device(): lax.all_to_all(shares, 'ep', split_axis=0, concat_axis=0, tiled=True)]
  transfers between devices with their start and end apart: 4 -> 6, of which waited for: 3 -> 6; matrix products, arithmetic and copies ran while one was open for 5% -> 5% of each run, Pallas kernels for 0% -> 0%
where the time goes in v1:
time: 172 us; the launch traced here: 171 us
  waiting for transfers between devices  92.7 us (54%)
  starting transfers between devices  18.3 us (11%)
  matrix products  17.5 us (10%)
  between operations  15.9 us (9%)
  blocking collectives  14.5 us (8%)
  local copies, waits for them, and re-layouts  7.54 us (4%)
  other arithmetic  4.98 us (3%)
    unnamed x3, waiting for transfers between devices  59.2 us
    psum x1, blocking collectives, on_device(): attn_out = lax.psum(partial_out, 'tp').astype(jnp.bfloat16)  14.5 us
    all_to_all x1, waiting for transfers between devices, on_device(): lax.all_to_all(dispatch, 'ep', split_axis=0, concat_axis=0, tiled=True)  13.4 us
    reduce_scatter x1, waiting for transfers between devices, on_device(): lax.psum_scatter(partial_units.astype(jnp.bfloat16), 'tp', scatter_dimens...  7.28 us
    all_to_all x1, waiting for transfers between devices, on_device(): lax.all_to_all(jnp.stack([own_hidden] * lax.axis_size('ep')), 'ep', 0, 0)  7.05 us
    all_to_all x1, starting transfers between devices, on_device(): lax.all_to_all(dispatch, 'ep', split_axis=0, concat_axis=0, tiled=True)  5.81 us
    all_to_all x1, starting transfers between devices, on_device(): lax.all_to_all(shares, 'ep', split_axis=0, concat_axis=0, tiled=True)  5.51 us
    dot_general x1, matrix products, on_device(): jnp.dot(dense_act, dense_down, preferred_element_type=jnp.float32)  3.83 us
  transfers between devices with their start and end apart: 6, of which 6 were waited for; matrix products, arithmetic and copies ran while one was open for 5% of the time, Pallas kernels for 0%

profile of v1, /device:TPU:0, one launch (start us, length us, event | category | flops | bytes accessed | tf_op | source)
XLA Modules:
  0.0 171.4 jit_solution(1168365458000044869)
XLA Ops:
  7.4 0.8 broadcast_add_fusion
  8.2 0.7 broadcast_compare_fusion
  8.8 0.7 iota_compare_fusion
  9.6 0.1 copy.44
  9.7 0.1 reshape.463
  9.8 0.0 copy-start.2
  9.9 1.8 %gather_fusion.2 = f32[32]{0:T(128)S(1)} fusion(f32[16,2,1024]{2,1,0:T(2,128)} %param.30, s32[32]{0:T(128)S(1)} %reshape.463), kind=kCustom, calls=%fused_computation.2 | custom fusion | bytes 640 | tf_op jit(solution)/shard_map/jit(take_along_axis)/gather | solution.py:86
  11.7 0.1 gather.13
  11.8 0.1 fusion.96
  11.9 0.0 copy-done.2
  11.9 0.1 fusion.72
  12.1 0.2 convolution_convert_fusion.3
  12.3 0.1 reshape.429
  12.4 0.2 fusion.101
  12.6 0.1 copy.45
  12.7 0.2 fusion.55
  12.9 0.2 fusion.54
  13.2 0.1 fusion.97
  13.3 3.6 %fusion.121 = (f32[16,2]{1,0:T(8,128)S(1)}, f32[16,2,1024]{2,1,0:T(2,128)S(1)}) fusion(f32[16,2]{1,0:T(8,128)S(1)} %copy.45, f32[16,2,1024]{2,1,0:T(2,128)S(1)} %copy-done.1, f32[16,2]{1,0:T(8,128)S(1)} %fusion.96, bf16[16,2,64]{2,1,0:T(2,128)(2,1)S(1)} %reshape.429, bf16[16,1024,1,128]{3,1,2,0:T(8,128)(2,1)} %param.29, ...), kind=kOutput, calls=%fused_computation.136 | convolution fusion | flops 4390880 | bytes 4477312 | tf_op jit(solution)/shard_map/skgd,slkd->skgl/dot_general | solution.py:80
  17.0 1.4 fusion.51
  18.4 0.1 reshape.432
  18.5 0.2 fusion.122
  18.7 14.5 %all-reduce.5 = bf16[16,2048]{1,0:T(8,128)(2,1)S(1)} all-reduce(f32[16,2048]{1,0:T(8,128)S(1)} %fusion.122), channel_id=1, replica_groups=mesh['ep'=8,'tp'=4] {'tp'}, use_global_device_ids=true, to_apply=%region_2.3 | all-reduce | flops 32768 | bytes 196608 | tf_op jit(solution)/shard_map/psum | solution.py:113
  33.2 0.1 multiply_reduce_fusion.1
  33.3 0.1 copy.48
  33.4 0.1 eq.37
  33.5 0.1 fusion.93
  33.6 0.1 copy.49
  33.7 0.1 reduce_window_sum.11
  33.8 0.2 select_reduce_fusion
  34.0 0.2 multiply_reduce_fusion.2
  34.2 0.1 reshape.433
  34.3 0.1 multiply_convert_fusion
  34.4 1.7 %gather_fusion = bf16[128,2048]{1,0:T(8,128)(2,1)} fusion(bf16[16,2048]{1,0:T(8,128)(2,1)S(1)} %multiply_convert_fusion, s32[1024]{0:T(1024)S(1)} %pad_clamp_fusion.1), kind=kCustom, calls=%fused_computation | custom fusion | bytes 1049088 | tf_op jit(solution)/shard_map/gather | solution.py:135
  36.1 5.8 %all-to-all-start = ((bf16[8,16,2048]{2,1,0:T(8,128)(2,1)}), bf16[8,16,2048]{2,1,0:T(8,128)(2,1)S(1)}, u32[]{:S(2)}, u32[]{:S(2)}) async-start(bf16[8,16,2048]{2,1,0:T(8,128)(2,1)} %bitcast.7), calls=%async_computation | async-start | bytes 1048576 | tf_op jit(solution)/shard_map/all_to_all | solution.py:136
  41.9 0.0 reduce-scatter.2.cloned.1.call-start
  42.0 13.4 %all-to-all-done = bf16[8,16,2048]{2,1,0:T(8,128)(2,1)S(1)} async-done(((bf16[8,16,2048]{2,1,0:T(8,128)(2,1)}), bf16[8,16,2048]{2,1,0:T(8,128)(2,1)S(1)}, u32[]{:S(2)}, u32[]{:S(2)}) %all-to-all-start) | async-done | bytes 524320 | tf_op jit(solution)/shard_map/all_to_all | solution.py:136
  55.4 2.0 %fusion.14 = f32[8,1,16,512]{3,2,0,1:T(8,128)S(1)} fusion(bf16[8,16,2048]{2,1,0:T(8,128)(2,1)S(1)} %all-to-all-done, bf16[1,2048,512]{2,1,0:T(8,128)(2,1)} %param.35), kind=kOutput, calls=%fused_computation.16 | convolution fusion | flops 268500992 | bytes 2883584 | tf_op jit(solution)/shard_map/sjnd,jdf->sjnf/dot_general | solution.py:139
  57.4 3.2 %convolution_convert_fusion = bf16[8,16,2048]{2,1,0:T(8,128)(2,1)} fusion(bf16[1,512,2048]{2,1,0:T(8,128)(2,1)S(1)} %copy-done, bf16[8,16,2048]{2,1,0:T(8,128)(2,1)S(1)} %all-to-all-done, bf16[1,2048,512]{2,1,0:T(8,128)(2,1)} %param.36, f32[8,1,16,512]{3,2,0,1:T(8,128)S(1)} %fusion.14), kind=kOutput, calls=%fused_computation.9 | convolution fusion | flops 537722880 | bytes 5505024 | tf_op jit(solution)/shard_map/sjnf,jfd->sjnd/dot_general | solution.py:144
  60.7 0.0 reduce-scatter.2.cloned.1.call-update
  60.7 0.7 stack.2
  61.4 3.7 %all-to-all-start.3 = ((bf16[8,4,2048]{2,1,0:T(4,128)(2,1)}), bf16[8,4,2048]{2,1,0:T(4,128)(2,1)S(1)}, u32[]{:S(2)}, u32[]{:S(2)}) async-start(bf16[8,4,2048]{2,1,0:T(4,128)(2,1)} %stack.2), calls=%async_computation.4 | async-start | bytes 262144 | tf_op jit(solution)/shard_map/all_to_all | solution.py:119
  65.1 0.1 reshape.440
  65.2 0.1 reshape.441
  65.3 0.1 copy.47
  65.4 7.0 %all-to-all-done.3 = bf16[8,4,2048]{2,1,0:T(4,128)(2,1)S(1)} async-done(((bf16[8,4,2048]{2,1,0:T(4,128)(2,1)}), bf16[8,4,2048]{2,1,0:T(4,128)(2,1)S(1)}, u32[]{:S(2)}, u32[]{:S(2)}) %all-to-all-start.3) | async-done | bytes 131104 | tf_op jit(solution)/shard_map/all_to_all | solution.py:119
  72.5 2.0 %convolution_minimum_fusion = f32[32,512]{1,0:T(8,128)S(1)} fusion(bf16[32,2048]{1,0:T(8,128)(2,1)S(1)} %reshape.442, bf16[2048,512]{1,0:T(8,128)(2,1)} %param.38), kind=kOutput, calls=%fused_computation.29 | convolution fusion | flops 67125248 | bytes 2293760 | tf_op jit(solution)/shard_map/dot_general | solution.py:121
  74.5 7.3 %reduce-scatter.2.cloned.1.call-done = bf16[8,16,512]{2,1,0:T(8,128)(2,1)} async-done(((bf16[8,16,2048]{2,1,0:T(8,128)(2,1)}), bf16[8,16,512]{2,1,0:T(8,128)(2,1)}) %reduce-scatter.2.cloned.1.call-update) | async-done | bytes 131088 | tf_op jit(solution)/shard_map/reduce_scatter | solution.py:149
  81.8 5.5 %all-to-all-start.1 = ((bf16[8,16,512]{2,1,0:T(8,128)(2,1)}), bf16[8,16,512]{2,1,0:T(8,128)(2,1)S(1)}, u32[]{:S(2)}, u32[]{:S(2)}) async-start(bf16[8,16,512]{2,1,0:T(8,128)(2,1)} %reduce-scatter.2.cloned.1.call-done), calls=%async_computation.2 | async-start | bytes 262144 | tf_op jit(solution)/shard_map/all_to_all | solution.py:152
  87.3 0.0 copy-start.15
  87.3 0.0 all-reduce.4.cloned.1.call-start
  87.4 3.8 %fusion.47 = f32[32,2048]{1,0:T(8,128)} fusion(bf16[512,2048]{1,0:T(8,128)(2,1)} %param.40, bf16[32,2048]{1,0:T(8,128)(2,1)S(1)} %reshape.442, bf16[2048,512]{1,0:T(8,128)(2,1)} %param.39, f32[32,512]{1,0:T(8,128)S(1)} %convolution_minimum_fusion), kind=kOutput, calls=%fused_computation.31 | convolution fusion | flops 134365184 | bytes 4653056 | tf_op jit(solution)/shard_map/dot_general | solution.py:125
  91.2 0.0 all-reduce.4.cloned.1.call-update
  91.2 3.4 %all-to-all-done.1 = bf16[8,16,512]{2,1,0:T(8,128)(2,1)S(1)} async-done(((bf16[8,16,512]{2,1,0:T(8,128)(2,1)}), bf16[8,16,512]{2,1,0:T(8,128)(2,1)S(1)}, u32[]{:S(2)}, u32[]{:S(2)}) %all-to-all-start.1) | async-done | bytes 131104 | tf_op jit(solution)/shard_map/all_to_all | solution.py:152
  94.7 0.7 gather_fusion.1
  95.4 0.2 multiply_reduce_fusion
  95.6 0.6 convert_element_type.115
  96.2 3.3 %all-to-all-start.2 = ((bf16[4,4,512]{2,1,0:T(4,128)(2,1)}), bf16[4,4,512]{2,1,0:T(4,128)(2,1)S(1)}, u32[]{:S(2)}, u32[]{:S(2)}) async-start(bf16[4,4,512]{2,1,0:T(4,128)(2,1)} %convert_element_type.115), calls=%async_computation.3 | async-start | bytes 32768 | tf_op jit(solution)/shard_map/all_to_all | solution.py:157
  99.5 0.1 fusion.60
  99.6 0.1 copy-done.15
  99.7 0.7 dynamic-slice
  101.0 2.3 %all-to-all-done.2 = bf16[4,4,512]{2,1,0:T(4,128)(2,1)S(1)} async-done(((bf16[4,4,512]{2,1,0:T(4,128)(2,1)}), bf16[4,4,512]{2,1,0:T(4,128)(2,1)S(1)}, u32[]{:S(2)}, u32[]{:S(2)}) %all-to-all-start.2) | async-done | bytes 16416 | tf_op jit(solution)/shard_map/all_to_all | solution.py:157
  103.3 59.2 %all-reduce.4.cloned.1.call-done = f32[32,2048]{1,0:T(8,128)} async-done(((f32[32,2048]{1,0:T(8,128)}), f32[32,2048]{1,0:T(8,128)}) %all-reduce.4.cloned.1.call-update) | async-done | bytes 262160
  162.5 1.5 fusion.88
  (47 shorter events, 0.3 us)
Async XLA Ops:
  7.4 50.1 %copy-start = (bf16[1,512,2048]{2,1,0:T(8,128)(2,1)S(1)}, bf16[1,512,2048]{2,1,0:T(8,128)(2,1)}, u32[]{:S(2)}) copy-start(bf16[1,512,2048]{2,1,0:T(8,128)(2,1)} %param.37) | copy-start | bytes 6291460
  9.8 2.1 %copy-start.2 = (bf16[16,2048]{1,0:T(8,128)(2,1)S(1)}, bf16[16,2048]{1,0:T(8,128)(2,1)}, u32[]{:S(2)}) copy-start(bf16[16,2048]{1,0:T(8,128)(2,1)} %param.21) | copy-start | bytes 196612
  9.8 2.2 %copy-start.4 = (bf16[2048,128]{1,0:T(8,128)(2,1)S(1)}, bf16[2048,128]{1,0:T(8,128)(2,1)}, u32[]{:S(2)}) copy-start(bf16[2048,128]{1,0:T(8,128)(2,1)} %param.23) | copy-start | bytes 1572868
  9.8 2.2 %copy-start.5 = (f32[2048]{0:T(1024)S(1)}, f32[2048]{0:T(1024)}, u32[]{:S(2)}) copy-start(f32[2048]{0:T(1024)} %param.22) | copy-start | bytes 24580
  9.9 2.5 %copy-start.12 = (bf16[2048,2]{0,1:T(2,128)(2,1)S(1)}, bf16[2048,2]{0,1:T(2,128)(2,1)}, u32[]{:S(2)}) copy-start(bf16[2048,2]{0,1:T(2,128)(2,1)} %param.26) | copy-start | bytes 24580
  9.9 2.5 %copy-start.14 = (f32[2]{0:T(128)S(1)}, f32[2]{0:T(128)}, u32[]{:S(2)}) copy-start(f32[2]{0:T(128)} %param.27) | copy-start | bytes 28
  9.9 2.8 %copy-start.10 = (bf16[2048,64]{0,1:T(8,128)(2,1)S(1)}, bf16[2048,64]{0,1:T(8,128)(2,1)}, u32[]{:S(2)}) copy-start(bf16[2048,64]{0,1:T(8,128)(2,1)} %param.24) | copy-start | bytes 786436
  9.9 3.0 %copy-start.11 = (bf16[2048,64]{0,1:T(8,128)(2,1)S(1)}, bf16[2048,64]{0,1:T(8,128)(2,1)}, u32[]{:S(2)}) copy-start(bf16[2048,64]{0,1:T(8,128)(2,1)} %param.25) | copy-start | bytes 786436
  9.9 3.4 %copy-start.1 = (f32[16,2,1024]{2,1,0:T(2,128)S(1)}, f32[16,2,1024]{2,1,0:T(2,128)}, u32[]{:S(2)}) copy-start(f32[16,2,1024]{2,1,0:T(2,128)} %param.30) | copy-start | bytes 393220
  13.3 3.7 %copy-start.9 = (bf16[16,1024,1,128]{3,1,2,0:T(8,128)(2,1)S(1)}, bf16[16,1024,1,128]{3,1,2,0:T(8,128)(2,1)}, u32[]{:S(2)}) copy-start(bf16[16,1024,1,128]{3,1,2,0:T(8,128)(2,1)} %param.29) | copy-start | bytes 12582916
  17.0 1.5 copy-start.3
  17.0 16.3 %copy-start.7 = (s32[16,4]{0,1:T(4,128)S(1)}, s32[16,4]{0,1:T(4,128)}, u32[]{:S(2)}) copy-start(s32[16,4]{0,1:T(4,128)} %param.33) | copy-start | bytes 772
  17.0 17.3 %copy-start.6 = (f32[2048]{0:T(1024)S(1)}, f32[2048]{0:T(1024)}, u32[]{:S(2)}) copy-start(f32[2048]{0:T(1024)} %param.32) | copy-start | bytes 24580
  36.1 19.3 %all-to-all-start = ((bf16[8,16,2048]{2,1,0:T(8,128)(2,1)}), bf16[8,16,2048]{2,1,0:T(8,128)(2,1)S(1)}, u32[]{:S(2)}, u32[]{:S(2)}) async-start(bf16[8,16,2048]{2,1,0:T(8,128)(2,1)} %bitcast.7), calls=%async_computation | async-start | bytes 1048576 | tf_op jit(solution)/shard_map/all_to_all | solution.py:136
  41.9 39.9 %reduce-scatter.2.cloned.1.call-start = ((), (), s32[]{:S(2)}) async-start(), calls=%async_computation.5 | async-start | bytes 655360 | tf_op jit(solution)/shard_map/reduce_scatter | solution.py:149
  57.4 7.9 %copy-start.8 = (f32[16,4]{0,1:T(4,128)S(1)}, f32[16,4]{0,1:T(4,128)}, u32[]{:S(2)}) copy-start(f32[16,4]{0,1:T(4,128)} %param.34) | copy-start | bytes 772
  61.4 11.0 %all-to-all-start.3 = ((bf16[8,4,2048]{2,1,0:T(4,128)(2,1)}), bf16[8,4,2048]{2,1,0:T(4,128)(2,1)S(1)}, u32[]{:S(2)}, u32[]{:S(2)}) async-start(bf16[8,4,2048]{2,1,0:T(4,128)(2,1)} %stack.2), calls=%async_computation.4 | async-start | bytes 262144 | tf_op jit(solution)/shard_map/all_to_all | solution.py:119
  81.8 12.9 %all-to-all-start.1 = ((bf16[8,16,512]{2,1,0:T(8,128)(2,1)}), bf16[8,16,512]{2,1,0:T(8,128)(2,1)S(1)}, u32[]{:S(2)}, u32[]{:S(2)}) async-start(bf16[8,16,512]{2,1,0:T(8,128)(2,1)} %reduce-scatter.2.cloned.1.call-done), calls=%async_computation.2 | async-start | bytes 262144 | tf_op jit(solution)/shard_map/all_to_all | solution.py:152
  87.3 12.1 %copy-start.13 = (f32[2048]{0:T(1024)S(1)}, f32[2048]{0:T(1024)}, u32[]{:S(2)}) copy-start(f32[2048]{0:T(1024)} %param.41) | copy-start | bytes 24580
  87.3 12.3 %copy-start.15 = (u32[32]{0:T(128)S(1)}, u32[32]{0:T(128)}, u32[]{:S(2)}) copy-start(u32[32]{0:T(128)} %constant.108) | copy-start | bytes 388
  87.3 75.1 %all-reduce.4.cloned.1.call-start = ((), (), s32[]{:S(2)}) async-start(), calls=%async_computation.6 | async-start | bytes 524288
  96.2 7.1 %all-to-all-start.2 = ((bf16[4,4,512]{2,1,0:T(4,128)(2,1)}), bf16[4,4,512]{2,1,0:T(4,128)(2,1)S(1)}, u32[]{:S(2)}, u32[]{:S(2)}) async-start(bf16[4,4,512]{2,1,0:T(4,128)(2,1)} %convert_element_type.115), calls=%async_computation.3 | async-start | bytes 32768 | tf_op jit(solution)/shard_map/all_to_all | solution.py:157
Sparse Core Ops, SparseCore 0:
  60.8 20.9 reduce-scatter.1
Sparse Core Ops, SparseCore 1:
  91.3 71.1 all-reduce.3
